TPU v7x, 32 devices: a whole 2x2x4 slice. The times are simulated.
32 devices in a mesh: row: 8 (over z, y), col: 4 (over x, core).
Axes of the slice: x: 2, y: 2, z: 4, core: 2. Of those that a mesh axis runs over, the one named last changes fastest.
Arguments:
- tokens: bfloat16 [16384, 2048], P(('row', 'col')), may hold values from -6 to 6
- w_mix: bfloat16 [2048, 512], replicated, may hold values from -0.125 to 0.125
- w_gate: bfloat16 [2048, 2048], replicated, may hold values from -0.125 to 0.125
- gate_bias: float32 [2048], replicated, may hold values from -4 to 4
- w_branch: bfloat16 [512, 2048], replicated, may hold values from -0.25 to 0.25
Outputs:
- mixed: bfloat16 [16384, 2048], P(('row', 'col'))
All inputs are finite; a program needn't handle non-finite values.
Results may differ from a plain program's by a relative error of at most 0.0083.
Values may be sent and summed in bfloat16 or wider, within the bound.
No kernel may reach another device: no remote copies, remote signals or barrier semaphores. Data moves between devices by JAX's collectives and lax.ppermute only.
A program may use at most 64 MiB of HBM per device.

v0:
```python
import math

import jax
import jax.numpy as jnp
from jax import lax
from jax.sharding import PartitionSpec as P

GROUP_DIM = 64


HIGH = lax.Precision.HIGHEST


def phase_table(left, right, period):
    product = left[:, None] * right[None, :] % period
    angle = product.astype(jnp.float32) * (2.0 * math.pi / period)
    return (jnp.cos(angle), jnp.sin(angle))


def group_tables(span):
    index = jnp.arange(span, dtype=jnp.int32)
    inner = index % GROUP_DIM
    cos_c, sin_c = phase_table(inner, inner, GROUP_DIM)
    same = (index[:, None] // GROUP_DIM == index[None, :] // GROUP_DIM).astype(jnp.float32)
    return (cos_c * same, sin_c * same)


def shards(tokens, w_mix, w_gate, gate_bias, w_branch):
    n_dev = lax.axis_size(("row", "col"))
    local_len = tokens.shape[0]
    full_len = local_len * n_dev
    sub_len = local_len // n_dev
    mixed_in = jnp.dot(tokens, w_mix, preferred_element_type=jnp.float32).astype(jnp.bfloat16)
    channels = mixed_in.shape[1]
    span = min(channels, max(GROUP_DIM, 128))
    pieces = lax.all_to_all(
        mixed_in.reshape(1, local_len, channels),
        ("row", "col"),
        split_axis=1,
        concat_axis=0,
        tiled=True,
    )
    values = pieces.astype(jnp.float32)
    dev_iota = jnp.arange(n_dev, dtype=jnp.int32)
    cos_p, sin_p = phase_table(dev_iota, dev_iota, n_dev)
    first_re = jnp.einsum("kn,nmc->kmc", cos_p, values, precision=HIGH)
    first_im = -jnp.einsum("kn,nmc->kmc", sin_p, values, precision=HIGH)
    cos_c, sin_c = group_tables(span)
    shaped = (n_dev, sub_len, channels // span, span)
    part_re = first_re.reshape(shaped)
    part_im = first_im.reshape(shaped)
    chan_re = jnp.einsum("kmgc,cd->kmgd", part_re, cos_c, precision=HIGH) + jnp.einsum(
        "kmgc,cd->kmgd", part_im, sin_c, precision=HIGH
    )
    chan_im = jnp.einsum("kmgc,cd->kmgd", part_im, cos_c, precision=HIGH) - jnp.einsum(
        "kmgc,cd->kmgd", part_re, sin_c, precision=HIGH
    )
    chan_re = chan_re.reshape(n_dev, sub_len, channels)
    chan_im = chan_im.reshape(n_dev, sub_len, channels)
    start = lax.axis_index(("row", "col")) * sub_len
    positions = start + jnp.arange(sub_len, dtype=jnp.int32)
    cos_t, sin_t = phase_table(dev_iota, positions, full_len)
    twist_re = chan_re * cos_t[:, :, None] + chan_im * sin_t[:, :, None]
    twist_im = chan_im * cos_t[:, :, None] - chan_re * sin_t[:, :, None]
    recv_re, recv_im = (
        lax.all_to_all(twist_re, ("row", "col"), split_axis=0, concat_axis=1, tiled=True),
        lax.all_to_all(twist_im, ("row", "col"), split_axis=0, concat_axis=1, tiled=True),
    )
    recv_re = recv_re.reshape(local_len, channels)
    recv_im = recv_im.reshape(local_len, channels)
    len_iota = jnp.arange(local_len, dtype=jnp.int32)
    cos_m, sin_m = phase_table(len_iota, len_iota, local_len)
    real_part = jnp.dot(cos_m, recv_re, precision=HIGH) + jnp.dot(sin_m, recv_im, precision=HIGH)
    real_part = real_part * (1.0 / math.sqrt(full_len * GROUP_DIM))
    freq_rows = real_part.astype(jnp.bfloat16).reshape(local_len, 1, channels)
    spectrum = lax.all_to_all(
        freq_rows, ("row", "col"), split_axis=0, concat_axis=1, tiled=True
    ).reshape(local_len, channels)
    gate = jax.nn.sigmoid(jnp.dot(tokens, w_gate, preferred_element_type=jnp.float32) + gate_bias)
    branch = jnp.dot(spectrum, w_branch, preferred_element_type=jnp.float32)
    return (gate * branch).astype(jnp.bfloat16)


def solution(mesh):
    in_specs = (P(("row", "col"), None), P(), P(), P(), P())
    out_specs = P(("row", "col"), None)
    return jax.shard_map(shards, mesh=mesh, in_specs=in_specs, out_specs=out_specs, check_vma=False)
```

profile of v0, /device:TPU:0, one launch (start us, length us, event | category | flops | bytes accessed | tf_op | source)
XLA Modules:
  0.0 156.2 jit_solution(4183638831278517337)
XLA Ops:
  0.0 1.6 %copy-done = bf16[512,2048]{1,0:T(8,128)(2,1)S(1)} copy-done((bf16[512,2048]{1,0:T(8,128)(2,1)S(1)}, bf16[512,2048]{1,0:T(8,128)(2,1)}, u32[]{:S(2)}) %copy-start) | copy-done | bytes 2097176
  1.6 2.8 %fusion.5 = bf16[1,512,512]{2,1,0:T(8,128)(2,1)S(1)} fusion(bf16[512,2048]{1,0:T(8,128)(2,1)S(1)} %copy-done, bf16[2048,512]{1,0:T(8,128)(2,1)} %param.6), kind=kOutput, calls=%fused_computation.14 | convolution fusion | flops 1074003968 | bytes 4718592 | tf_op jit(solution)/shard_map/dot_general | solution.py:33
  4.4 0.8 copy.68
  5.8 4.6 %reduce = bf16[512,512]{1,0:T(8,128)(2,1)} reduce(bf16[512,1,512]{2,1,0:T(2,128)(2,1)S(1)} %bitcast.70, bf16[]{:T(256)} %broadcast.262), dimensions={1}, to_apply=%bitcast.66.reduce_sub_computation | reduce | bytes 1048578
  10.4 2.2 %reshape.199 = bf16[32,2,4096]{2,1,0:T(2,128)(2,1)} reshape(bf16[512,512]{1,0:T(8,128)(2,1)} %reduce) | data formatting | bytes 1048576
  12.7 7.5 %all-to-all-start = ((bf16[32,2,4096]{2,1,0:T(2,128)(2,1)}), bf16[32,2,4096]{2,1,0:T(2,128)(2,1)S(1)}, u32[]{:S(2)}, u32[]{:S(2)}) async-start(bf16[32,2,4096]{2,1,0:T(2,128)(2,1)} %reshape.199), calls=%async_computation | async-start | bytes 1048576 | tf_op jit(solution)/shard_map/all_to_all | solution.py:36
  20.3 15.3 %all-to-all-done = bf16[32,2,4096]{2,1,0:T(2,128)(2,1)S(1)} async-done(((bf16[32,2,4096]{2,1,0:T(2,128)(2,1)}), bf16[32,2,4096]{2,1,0:T(2,128)(2,1)S(1)}, u32[]{:S(2)}, u32[]{:S(2)}) %all-to-all-start) | async-done | bytes 524320 | tf_op jit(solution)/shard_map/all_to_all | solution.py:36
  35.6 1.8 %reshape.200 = bf16[512,1,512]{2,1,0:T(2,128)(2,1)} reshape(bf16[32,2,4096]{2,1,0:T(2,128)(2,1)S(1)} %all-to-all-done) | data formatting | bytes 1048576
  37.4 1.3 copy.47
  38.8 0.8 copy-done.2
  39.5 0.9 reshape.198
  40.5 1.8 %fusion.23 = f32[32,16,4,128]{3,0,2,1:T(8,128)S(1)} fusion(bf16[16,4,128,32]{2,1,0,3:T(4,128)(2,1)} %reshape.198), kind=kOutput, calls=%fused_computation.36 | convolution fusion | flops 100677632 | bytes 1572864 | tf_op jit(solution)/shard_map/kn,nmc->kmc/dot_general | solution.py:46
  42.3 2.9 %convolution_negate_fusion = f32[32,16,512]{2,0,1:T(8,128)} fusion(bf16[32,16,512]{2,1,0:T(8,128)(2,1)} %bitcast.68), kind=kOutput, calls=%fused_computation.4 | convolution fusion | flops 100939776 | bytes 1572864 | tf_op jit(solution)/shard_map/kn,nmc->kmc/dot_general | solution.py:47
  45.1 2.5 %reshape.187 = f32[32,16,4,128]{3,2,0,1:T(4,128)} reshape(f32[32,16,512]{2,0,1:T(8,128)} %convolution_negate_fusion) | data formatting | bytes 2097152 | tf_op jit(solution)/shard_map/reshape | solution.py:51
  47.7 2.0 %fusion.21 = f32[32,16,4,128]{3,1,2,0:T(8,128)S(1)} fusion(f32[32,16,4,128]{3,0,2,1:T(8,128)S(1)} %fusion.23, s32[128]{0:T(128)S(1)} %get-tuple-element.9, s32[128]{0:T(128)S(1)} %get-tuple-element.10), kind=kOutput, calls=%fused_computation.34 | convolution fusion | flops 402915328 | bytes 2098176 | tf_op jit(solution)/shard_map/kmgc,cd->kmgd/dot_general | solution.py:52
  49.7 1.8 %fusion.17 = f32[32,16,4,128]{3,1,2,0:T(8,128)S(1)} fusion(f32[32,16,4,128]{3,2,0,1:T(4,128)S(1)} %copy-done.1, s32[128]{0:T(128)S(1)} %get-tuple-element.9, s32[128]{0:T(128)S(1)} %get-tuple-element.10), kind=kOutput, calls=%fused_computation.30 | convolution fusion | flops 402915328 | bytes 2098176 | tf_op jit(solution)/shard_map/kmgc,cd->kmgd/dot_general | solution.py:55
  51.5 1.8 %fusion.2 = f32[32,4,2,8,128]{4,3,2,1,0:T(8,128)S(1)} fusion(f32[32,16,4,128]{3,1,2,0:T(8,128)S(1)} %fusion.21, f32[32,16,4,128]{3,2,0,1:T(4,128)S(1)} %copy-done.1, s32[128]{0:T(128)S(1)} %get-tuple-element.9, s32[128]{0:T(128)S(1)} %get-tuple-element.10), kind=kOutput, calls=%fused_computation.10 | convolution fusion | flops 403177472 | bytes 3146752 | tf_op jit(solution)/shard_map/kmgc,cd->kmgd/dot_general | solution.py:52
  53.3 2.0 %fusion.1 = f32[32,4,2,8,128]{4,3,2,1,0:T(8,128)S(1)} fusion(f32[32,16,4,128]{3,1,2,0:T(8,128)S(1)} %fusion.17, f32[32,16,4,128]{3,0,2,1:T(8,128)S(1)} %fusion.23, s32[128]{0:T(128)S(1)} %get-tuple-element.9, s32[128]{0:T(128)S(1)} %get-tuple-element.10), kind=kOutput, calls=%fused_computation.8 | convolution fusion | flops 403177472 | bytes 3146752 | tf_op jit(solution)/shard_map/kmgc,cd->kmgd/dot_general | solution.py:55
  55.4 1.3 fusion.10
  56.6 29.1 %all_to_all.45 = f32[32,16,512]{2,1,0:T(8,128)} all-to-all(f32[32,16,512]{2,1,0:T(8,128)S(1)} %get-tuple-element.6), channel_id=1, replica_groups=mesh['row'=8,'col'=4] {'row','col'}, dimensions={0} | all-to-all | bytes 2097152 | tf_op jit(solution)/shard_map/all_to_all | solution.py:66
  85.7 3.8 %all-to-all-start.2 = ((f32[32,16,512]{2,1,0:T(8,128)}), f32[32,16,512]{2,1,0:T(8,128)S(1)}, u32[]{:S(2)}, u32[]{:S(2)}) async-start(f32[32,16,512]{2,1,0:T(8,128)} %get-tuple-element.5), calls=%async_computation.2 | async-start | bytes 2097152 | tf_op jit(solution)/shard_map/all_to_all | solution.py:67
  89.6 8.0 %fusion.12 = f32[512,512]{1,0:T(8,128)} fusion(f32[512,512]{1,0:T(8,128)} %bitcast.73), kind=kOutput, calls=%fused_computation.25 | convolution fusion | flops 1614282752 | bytes 2097152 | tf_op jit(solution)/shard_map/dot_general | solution.py:73
  97.5 18.0 %all-to-all-done.2 = f32[32,16,512]{2,1,0:T(8,128)S(1)} async-done(((f32[32,16,512]{2,1,0:T(8,128)}), f32[32,16,512]{2,1,0:T(8,128)S(1)}, u32[]{:S(2)}, u32[]{:S(2)}) %all-to-all-start.2) | async-done | bytes 1048608 | tf_op jit(solution)/shard_map/all_to_all | solution.py:67
  115.6 7.8 %fusion.4 = bf16[512,1,512]{2,0,1:T(8,128)(2,1)} fusion(f32[512,512]{1,0:T(8,128)} %fusion.12, f32[512,512]{1,0:T(8,128)S(1)} %bitcast.72), kind=kOutput, calls=%fused_computation.13 | convolution fusion | flops 1615069184 | bytes 2621440 | tf_op jit(solution)/shard_map/dot_general | solution.py:73
  123.4 2.1 %reduce.1 = bf16[512,512]{1,0:T(8,128)(2,1)S(1)} reduce(bf16[512,1,512]{2,0,1:T(8,128)(2,1)} %fusion.4, bf16[]{:T(256)} %broadcast.262), dimensions={1}, to_apply=%copy.40.reduce_sub_computation | reduce | bytes 1048578 | tf_op jit(solution)/shard_map/reshape | solution.py:75
  125.5 1.2 reshape.201
  126.6 4.0 %all-to-all-start.3 = ((bf16[32,2,4096]{2,1,0:T(2,128)(2,1)}), bf16[32,2,4096]{2,1,0:T(2,128)(2,1)}, u32[]{:S(2)}, u32[]{:S(2)}) async-start(bf16[32,2,4096]{2,1,0:T(2,128)(2,1)} %reshape.201), calls=%async_computation.3 | async-start | bytes 1048576 | tf_op jit(solution)/shard_map/all_to_all | solution.py:76
  130.6 9.4 %fusion.109 = f32[512,2048]{1,0:T(8,128)} fusion(bf16[512,2048]{1,0:T(8,128)(2,1)S(1)} %copy-done, bf16[2048,2048]{1,0:T(8,128)(2,1)} %param.7), kind=kOutput, calls=%fused_computation.130 | convolution fusion | flops 4294967296 | bytes 14680064 | tf_op jit(solution)/shard_map/dot_general | solution.py:79
  140.0 6.0 %all-to-all-done.3 = bf16[32,2,4096]{2,1,0:T(2,128)(2,1)} async-done(((bf16[32,2,4096]{2,1,0:T(2,128)(2,1)}), bf16[32,2,4096]{2,1,0:T(2,128)(2,1)}, u32[]{:S(2)}, u32[]{:S(2)}) %all-to-all-start.3) | async-done | bytes 524320 | tf_op jit(solution)/shard_map/all_to_all | solution.py:76
  146.0 3.6 %reshape.202 = bf16[512,1,512]{2,1,0:T(2,128)(2,1)S(1)} reshape(bf16[32,2,4096]{2,1,0:T(2,128)(2,1)} %all-to-all-done.3) | data formatting | bytes 1048576
  150.1 1.1 copy-done.3
  151.2 5.0 %multiply_convert_fusion = bf16[512,2048]{1,0:T(8,128)(2,1)} fusion(f32[512,2048]{1,0:T(8,128)} %fusion.109, bf16[512,512]{1,0:T(8,128)(2,1)S(1)} %bitcast.74, bf16[512,2048]{1,0:T(8,128)(2,1)S(1)} %copy-done.3, f32[2048]{0:T(1024)S(1)} %copy-done.4), kind=kOutput, calls=%fused_computation | convolution fusion | flops 1080033280 | bytes 8921088 | tf_op jit(solution)/shard_map/dot_general | solution.py:80
  (13 shorter events, 1.1 us)
Async XLA Ops:
  0.0 1.6 %copy-start = (bf16[512,2048]{1,0:T(8,128)(2,1)S(1)}, bf16[512,2048]{1,0:T(8,128)(2,1)}, u32[]{:S(2)}) copy-start(bf16[512,2048]{1,0:T(8,128)(2,1)} %param.5) | copy-start | bytes 6291460
  12.7 22.9 %all-to-all-start = ((bf16[32,2,4096]{2,1,0:T(2,128)(2,1)}), bf16[32,2,4096]{2,1,0:T(2,128)(2,1)S(1)}, u32[]{:S(2)}, u32[]{:S(2)}) async-start(bf16[32,2,4096]{2,1,0:T(2,128)(2,1)} %reshape.199), calls=%async_computation | async-start | bytes 1048576 | tf_op jit(solution)/shard_map/all_to_all | solution.py:36
  38.7 0.8 copy-start.2
  47.7 2.0 %copy-start.1 = (f32[32,16,4,128]{3,2,0,1:T(4,128)S(1)}, f32[32,16,4,128]{3,2,0,1:T(4,128)}, u32[]{:S(2)}) copy-start(f32[32,16,4,128]{3,2,0,1:T(4,128)} %reshape.187) | copy-start | bytes 3145732
  85.7 29.8 %all-to-all-start.2 = ((f32[32,16,512]{2,1,0:T(8,128)}), f32[32,16,512]{2,1,0:T(8,128)S(1)}, u32[]{:S(2)}, u32[]{:S(2)}) async-start(f32[32,16,512]{2,1,0:T(8,128)} %get-tuple-element.5), calls=%async_computation.2 | async-start | bytes 2097152 | tf_op jit(solution)/shard_map/all_to_all | solution.py:67
  126.6 19.3 %all-to-all-start.3 = ((bf16[32,2,4096]{2,1,0:T(2,128)(2,1)}), bf16[32,2,4096]{2,1,0:T(2,128)(2,1)}, u32[]{:S(2)}, u32[]{:S(2)}) async-start(bf16[32,2,4096]{2,1,0:T(2,128)(2,1)} %reshape.201), calls=%async_computation.3 | async-start | bytes 1048576 | tf_op jit(solution)/shard_map/all_to_all | solution.py:76
  140.0 10.0 %copy-start.4 = (f32[2048]{0:T(1024)S(1)}, f32[2048]{0:T(1024)}, u32[]{:S(2)}) copy-start(f32[2048]{0:T(1024)} %param.8) | copy-start | bytes 24580
  149.6 1.6 %copy-start.3 = (bf16[512,2048]{1,0:T(8,128)(2,1)S(1)}, bf16[512,2048]{1,0:T(8,128)(2,1)}, u32[]{:S(2)}) copy-start(bf16[512,2048]{1,0:T(8,128)(2,1)} %param.9) | copy-start | bytes 6291460
where the time goes:
time: 157 us; the launch traced here: 156 us
  matrix products  45.3 us (29%)
  waiting for transfers between devices  39.3 us (25%)
  blocking collectives  29.1 us (19%)
  local copies, waits for them, and re-layouts  18.9 us (12%)
  starting transfers between devices  15.4 us (10%)
  other arithmetic  8.03 us (5%)
    all_to_all x1, blocking collectives, shards(): lax.all_to_all(twist_re, ('row', 'col'), split_axis=0, concat_axis=1, til...  29.1 us
    all_to_all x1, waiting for transfers between devices, shards(): lax.all_to_all(twist_im, ('row', 'col'), split_axis=0, concat_axis=1, til...  18 us
    all_to_all x1, waiting for transfers between devices, shards(): lax.all_to_all(mixed_in.reshape(1, local_len, channels), ('row', 'col'),...  15.3 us
    unnamed x17, local copies, waits for them, and re-layouts  14.4 us
    dot_general x1, matrix products, shards(): jnp.dot(tokens, w_gate, preferred_element_type=jnp.float32) + gate_bias  9.37 us
    dot_general x1, matrix products, shards(): jnp.dot(cos_m, recv_re, precision=HIGH)  7.95 us
    dot_general x1, matrix products, shards(): jnp.dot(sin_m, recv_im, precision=HIGH)  7.84 us
    all_to_all x1, starting transfers between devices, shards(): lax.all_to_all(mixed_in.reshape(1, local_len, channels), ('row', 'col'),...  7.51 us
  transfers between devices with their start and end apart: 3, of which 3 were waited for; matrix products, arithmetic and copies ran while one was open for 11% of the time, Pallas kernels for 0%

commit v1 on v0

v1 whole, which is shorter than its diff:
```python
import functools
import math

import jax
import jax.numpy as jnp
import numpy as np
from jax import lax
from jax.experimental import pallas as pl
from jax.experimental.pallas import tpu as pltpu
from jax.sharding import PartitionSpec as P

GROUP_DIM = 64
LANES = 128
AXES = ("row", "col")


def wave(left, right, period):
    angle = (np.outer(left, right) % period) * (2.0 * np.pi / period)
    return np.cos(angle), np.sin(angle)


def channel_tables(channels, n_dev):
    slots = channels // n_dev
    pairs = slots // 2
    half = GROUP_DIM // 2
    index = np.arange(GROUP_DIM)
    forward = np.zeros((channels, channels))
    combine = np.zeros((channels, channels))
    for q in range(channels // 2):
        group, d = divmod(q, half)
        base = group * GROUP_DIM
        even = (q // pairs) * slots + q % pairs
        odd = even + pairs
        rows = slice(base, base + GROUP_DIM)
        forward[rows, even] = np.cos(2 * np.pi * (index * d % GROUP_DIM) / GROUP_DIM)
        if d == 0:
            forward[rows, odd] = np.cos(np.pi * index)
            combine[even, base] = 1.0
            combine[odd, base + half] = 1.0
        else:
            forward[rows, odd] = np.sin(2 * np.pi * (index * d % GROUP_DIM) / GROUP_DIM)
            combine[even, base + d] = 1.0
            combine[odd, base + d] = 1.0
            combine[even, base + GROUP_DIM - d] = 1.0
            combine[odd, base + GROUP_DIM - d] = -1.0
    return forward / math.sqrt(GROUP_DIM), combine


def length_tables(n_dev, local_len, slots):
    full_len = n_dev * local_len
    sub = local_len // n_dev
    dev = np.arange(n_dev)
    pos = np.arange(local_len)
    eye = np.eye(slots)
    cos_j, sin_j = wave(dev, dev, n_dev)
    first = np.concatenate(
        [
            np.einsum("cj,st->scjt", table, eye).reshape(slots * n_dev, n_dev * slots)
            for table in (cos_j, -sin_j)
        ]
    )
    cos_t, sin_t = wave(dev, pos, full_len)
    v_n = local_len // LANES
    u_n = sub // v_n
    v, u, big = np.meshgrid(np.arange(v_n), np.arange(u_n), dev, indexing="ij")
    freq = (big * sub + u * v_n + v).reshape(-1)
    cos_m, sin_m = wave(freq, pos, local_len)
    last = np.concatenate([cos_m, sin_m], axis=1) / math.sqrt(full_len)
    f_n = slots // v_n
    source = np.arange(local_len).reshape(v_n, f_n, n_dev).transpose(1, 0, 2).reshape(-1)
    lane_perm = np.zeros((local_len, local_len))
    lane_perm[source, np.arange(local_len)] = 1.0
    source = np.arange(slots * n_dev).reshape(slots, n_dev).T.reshape(-1)
    row_perm = np.zeros((slots * n_dev, slots * n_dev))
    row_perm[np.arange(slots * n_dev), source] = 1.0
    return first, cos_t, sin_t, last, lane_perm, row_perm


def length_kernel(n_dev, slots, flag_ref, x_ref, first_ref, cos_ref, sin_ref, last_ref, lane_ref, row_ref, out_ref, z_ref, a_ref, b_ref):
    rows, lanes = x_ref.shape
    pairs = slots // 2
    f32 = jnp.float32
    y_re = jnp.dot(first_ref[:rows, :], x_ref[...], preferred_element_type=f32)
    y_im = jnp.dot(first_ref[rows:, :], x_ref[...], preferred_element_type=f32)
    cos_t, sin_t = cos_ref[...], sin_ref[...]
    flag = flag_ref[0]
    for slot in range(slots):
        if slot < pairs:
            t_re, t_im = cos_t, -sin_t
        elif slot == pairs:
            t_re = flag * cos_t - (1.0 - flag) * sin_t
            t_im = -flag * sin_t - (1.0 - flag) * cos_t
        else:
            t_re, t_im = -sin_t, -cos_t
        here = slice(slot * n_dev, (slot + 1) * n_dev)
        p_re, p_im = y_re[here, :], y_im[here, :]
        z_ref[here, :lanes] = (p_re * t_re - p_im * t_im).astype(jnp.bfloat16)
        z_ref[here, lanes:] = (p_re * t_im + p_im * t_re).astype(jnp.bfloat16)
    spec = lax.dot_general(last_ref[...], z_ref[...], (((1,), (1,)), ((), ())), preferred_element_type=f32)
    spec = spec.astype(jnp.bfloat16)
    blocks = lanes // LANES
    tall = rows // blocks
    for e in range(blocks):
        for v in range(blocks):
            a_ref[e * tall : (e + 1) * tall, v * LANES : (v + 1) * LANES] = spec[
                v * tall : (v + 1) * tall, e * LANES : (e + 1) * LANES
            ]
    f_n = slots // blocks
    if f_n > 1:
        mixed = jnp.dot(a_ref[...], lane_ref[...], preferred_element_type=f32).astype(jnp.bfloat16)
        wide = lanes // f_n
        for e in range(blocks):
            for f in range(f_n):
                for u in range(f_n):
                    low, high = e * tall + f * n_dev, e * tall + u * n_dev
                    b_ref[low : low + n_dev, u * wide : (u + 1) * wide] = mixed[
                        high : high + n_dev, f * wide : (f + 1) * wide
                    ]
        ordered = b_ref[...]
    else:
        ordered = a_ref[...]
    out_ref[...] = jnp.dot(row_ref[...], ordered, preferred_element_type=f32).astype(jnp.bfloat16)


def shards(tokens, w_mix, w_gate, gate_bias, w_branch):
    n_dev = lax.axis_size(AXES)
    local_len = tokens.shape[0]
    channels = w_mix.shape[1]
    slots = channels // n_dev
    pairs = slots // 2
    bf16, f32 = jnp.bfloat16, jnp.float32
    assert channels == local_len and slots % (local_len // LANES) == 0
    assert (GROUP_DIM // 2) % pairs == 0
    forward, combine = channel_tables(channels, n_dev)
    tables = length_tables(n_dev, local_len, slots)
    first, cos_t, sin_t, last, lane_perm, row_perm = (
        jnp.asarray(t, dtype) for t, dtype in zip(tables, (bf16, f32, f32, bf16, bf16, bf16))
    )
    mixed_in = jnp.dot(tokens, w_mix, preferred_element_type=f32).astype(bf16)
    slotted = lax.dot_general(
        jnp.asarray(forward, bf16), mixed_in, (((0,), (1,)), ((), ())), preferred_element_type=f32
    ).astype(bf16)
    pieces = lax.all_to_all(
        slotted.reshape(n_dev, slots, local_len), AXES, split_axis=0, concat_axis=0, tiled=True
    ).reshape(channels, local_len)
    flag = (lax.axis_index(AXES) * pairs % (GROUP_DIM // 2) == 0).astype(f32).reshape(1)
    vmem = pl.BlockSpec(memory_space=pltpu.VMEM)
    spectra = pl.pallas_call(
        functools.partial(length_kernel, n_dev, slots),
        out_shape=jax.ShapeDtypeStruct((channels, local_len), bf16),
        in_specs=[pl.BlockSpec(memory_space=pltpu.SMEM)] + [vmem] * 7,
        out_specs=vmem,
        scratch_shapes=[
            pltpu.VMEM((channels, 2 * local_len), bf16),
            pltpu.VMEM((channels, local_len), bf16),
            pltpu.VMEM((channels, local_len), bf16),
        ],
        cost_estimate=pl.CostEstimate(
            flops=12 * channels * local_len * local_len, bytes_accessed=6 << 20, transcendentals=0
        ),
        name="length_transform",
    )(flag, pieces, first, cos_t, sin_t, last, lane_perm, row_perm)
    back = lax.all_to_all(
        spectra.reshape(n_dev, slots, local_len), AXES, split_axis=0, concat_axis=0, tiled=True
    ).reshape(channels, local_len)
    gate = jax.nn.sigmoid(jnp.dot(tokens, w_gate, preferred_element_type=f32) + gate_bias)
    spectrum = lax.dot_general(
        back, jnp.asarray(combine, bf16), (((0,), (0,)), ((), ())), preferred_element_type=f32
    ).astype(bf16)
    branch = jnp.dot(spectrum, w_branch, preferred_element_type=f32)
    return (gate * branch).astype(bf16)


def solution(mesh):
    in_specs = (P(AXES, None), P(), P(), P(), P())
    out_specs = P(AXES, None)
    return jax.shard_map(shards, mesh=mesh, in_specs=in_specs, out_specs=out_specs, check_vma=False)
```

time: 157 us -> 58.7 us (0.37)
  blocking collectives: 29.1 us -> 0 us
  matrix products: 45.3 us -> 18.8 us
  waiting for transfers between devices: 39.3 us -> 21.8 us
  local copies, waits for them, and re-layouts: 18.9 us -> 2.4 us
  other arithmetic: 8.03 us -> 0 us
  starting transfers between devices: 15.4 us -> 10.3 us
  Pallas kernels: 0 us -> 5 us
    all_to_all x1 -> x0, blocking collectives: 29.1 us -> none  [shards(): lax.all_to_all(twist_re, ('row', 'col'), split_axis=0, concat_axis=1, til...]
    dot_general x11 -> x3, matrix products: 45.3 us -> 18.8 us  [the longest x1 9.43 us: shards(): jnp.dot(tokens, w_gate, preferred_element_type=f32) + gate_bias]
    all_to_all x3 -> x2, waiting for transfers between devices: 39.3 us -> 21.8 us  [the longest x1 15.6 us: shards(): lax.all_to_all(slotted.reshape(n_dev, slots, local_len), AXES, split_axis...]
    unnamed x17 -> x8, local copies, waits for them, and re-layouts: 14.4 us -> 2.4 us
    all_to_all x3 -> x2, starting transfers between devices: 15.4 us -> 10.3 us  [the longest x1 7.32 us: shards(): lax.all_to_all(slotted.reshape(n_dev, slots, local_len), AXES, split_axis...]
    pallas_call x0 -> x1, Pallas kernels: none -> 5 us  [shards(): pl.pallas_call(functools.partial(length_kernel, n_dev, slots), out_shape=...]
    unnamed x1 -> x0, other arithmetic: 4.6 us -> none
    reshape x2 -> x0, local copies, waits for them, and re-layouts: 3.34 us -> none  [the longest x1 2.53 us: shards(): part_im = first_im.reshape(shaped)]
  transfers between devices with their start and end apart: 3 -> 2, of which waited for: 3 -> 2; matrix products, arithmetic and copies ran while one was open for 11% -> 16% of each run, Pallas kernels for 0% -> 0%
where the time goes in v1:
time: 58.7 us; the launch traced here: 58.3 us
  waiting for transfers between devices  21.8 us (37%)
  matrix products  18.8 us (32%)
  starting transfers between devices  10.3 us (18%)
  Pallas kernels  5 us (9%)
  local copies, waits for them, and re-layouts  2.4 us (4%)
    all_to_all x1, waiting for transfers between devices, shards(): lax.all_to_all(slotted.reshape(n_dev, slots, local_len), AXES, split_axis...  15.6 us
    dot_general x1, matrix products, shards(): jnp.dot(tokens, w_gate, preferred_element_type=f32) + gate_bias  9.43 us
    all_to_all x1, starting transfers between devices, shards(): lax.all_to_all(slotted.reshape(n_dev, slots, local_len), AXES, split_axis...  7.32 us
    all_to_all x1, waiting for transfers between devices, shards(): lax.all_to_all(spectra.reshape(n_dev, slots, local_len), AXES, split_axis...  6.16 us
    dot_general x1, matrix products, shards(): branch = jnp.dot(spectrum, w_branch, preferred_element_type=f32)  5.27 us
    pallas_call x1, Pallas kernels, shards(): pl.pallas_call(functools.partial(length_kernel, n_dev, slots), out_shape=...  5 us
    dot_general x1, matrix products, shards(): lax.dot_general(jnp.asarray(forward, bf16), mixed_in, (((0,), (1,)), ((),...  4.1 us
    all_to_all x1, starting transfers between devices, shards(): lax.all_to_all(spectra.reshape(n_dev, slots, local_len), AXES, split_axis...  2.97 us
  transfers between devices with their start and end apart: 2, of which 2 were waited for; matrix products, arithmetic and copies ran while one was open for 16% of the time, Pallas kernels for 0%

profile of v1, /device:TPU:0, one launch (start us, length us, event | category | flops | bytes accessed | tf_op | source)
XLA Modules:
  0.0 58.3 jit_solution(15131183995115165362)
XLA Ops:
  0.0 0.0 copy-start
  0.0 1.6 %copy-done = bf16[512,2048]{1,0:T(8,128)(2,1)S(1)} copy-done((bf16[512,2048]{1,0:T(8,128)(2,1)S(1)}, bf16[512,2048]{1,0:T(8,128)(2,1)}, u32[]{:S(2)}) %copy-start) | copy-done | bytes 2097176
  1.6 4.1 %convolution_convert_fusion.1 = bf16[512,512]{0,1:T(8,128)(2,1)} fusion(bf16[512,512]{1,0:T(8,128)(2,1)} %constant.51.clone, bf16[512,2048]{1,0:T(8,128)(2,1)S(1)} %copy-done, bf16[2048,512]{1,0:T(8,128)(2,1)} %param.14), kind=kOutput, calls=%fused_computation.2 | convolution fusion | flops 1342701568 | bytes 5242880 | tf_op jit(solution)/shard_map/dot_general | solution.py:140
  5.7 7.3 %all-to-all-start = ((bf16[32,16,512]{2,1,0:T(8,128)(2,1)}), bf16[32,16,512]{2,1,0:T(8,128)(2,1)S(1)}, u32[]{:S(2)}, u32[]{:S(2)}) async-start(bf16[32,16,512]{2,1,0:T(8,128)(2,1)} %bitcast.2), calls=%async_computation | async-start | bytes 1048576 | tf_op jit(solution)/shard_map/all_to_all | solution.py:143
  13.0 15.6 %all-to-all-done = bf16[32,16,512]{2,1,0:T(8,128)(2,1)S(1)} async-done(((bf16[32,16,512]{2,1,0:T(8,128)(2,1)}), bf16[32,16,512]{2,1,0:T(8,128)(2,1)S(1)}, u32[]{:S(2)}, u32[]{:S(2)}) %all-to-all-start) | async-done | bytes 524320 | tf_op jit(solution)/shard_map/all_to_all | solution.py:143
  28.6 0.0 copy-start.1
  28.6 0.8 %copy-done.1 = bf16[32,16,512]{2,1,0:T(8,128)(2,1)} copy-done((bf16[32,16,512]{2,1,0:T(8,128)(2,1)}, bf16[32,16,512]{2,1,0:T(8,128)(2,1)S(1)}, u32[]{:S(2)}) %copy-start.1) | copy-done | bytes 524312
  29.4 5.0 %length_transform.1 = bf16[512,512]{1,0:T(8,128)(2,1)} custom-call(f32[1]{0:T(128)} %bitcast.flag_ref, bf16[512,512]{1,0:T(8,128)(2,1)} %bitcast.15, bf16[1024,512]{1,0:T(8,128)(2,1)} %constant.45.clone.first_ref, f32[32,512]{1,0:T(8,128)} %constant.46.clone.cos_ref, f32[32,512]{1,0:T(8,128)} %constant.47.clone.sin_ref, ...), custom_call_target="tpu_custom_call" | custom-call | flops 1610612736 | bytes 6291456 | tf_op jit(solution)/shard_map/length_transform/pallas_call | solution.py:148
  34.4 3.0 %all-to-all-start.1 = ((bf16[32,16,512]{2,1,0:T(8,128)(2,1)}), bf16[32,16,512]{2,1,0:T(8,128)(2,1)S(1)}, u32[]{:S(2)}, u32[]{:S(2)}) async-start(bf16[32,16,512]{2,1,0:T(8,128)(2,1)} %bitcast.16), calls=%async_computation.1 | async-start | bytes 1048576 | tf_op jit(solution)/shard_map/all_to_all | solution.py:163
  37.4 0.0 copy-start.2
  37.4 0.0 copy-start.3
  37.4 9.4 %fusion = f32[512,2048]{1,0:T(8,128)} fusion(bf16[512,2048]{1,0:T(8,128)(2,1)S(1)} %copy-done, bf16[2048,2048]{1,0:T(8,128)(2,1)} %param.15), kind=kOutput, calls=%fused_computation.4 | convolution fusion | flops 4294967296 | bytes 14680064 | tf_op jit(solution)/shard_map/dot_general | solution.py:166
  46.9 6.2 %all-to-all-done.1 = bf16[32,16,512]{2,1,0:T(8,128)(2,1)S(1)} async-done(((bf16[32,16,512]{2,1,0:T(8,128)(2,1)}), bf16[32,16,512]{2,1,0:T(8,128)(2,1)S(1)}, u32[]{:S(2)}, u32[]{:S(2)}) %all-to-all-start.1) | async-done | bytes 524320 | tf_op jit(solution)/shard_map/all_to_all | solution.py:163
  53.0 0.0 copy-done.2
  53.0 0.0 copy-done.3
  53.0 5.3 %multiply_convert_fusion = bf16[512,2048]{1,0:T(8,128)(2,1)} fusion(f32[512,2048]{1,0:T(8,128)} %fusion, bf16[512,2048]{1,0:T(8,128)(2,1)} %param.17, f32[2048]{0:T(1024)S(1)} %copy-done.2, bf16[512,512]{1,0:T(8,128)(2,1)S(1)} %bitcast.17, bf16[512,512]{1,0:T(8,128)(2,1)S(1)} %copy-done.3), kind=kOutput, calls=%fused_computation | convolution fusion | flops 1348730880 | bytes 9445376 | tf_op jit(solution)/shard_map/dot_general | solution.py:170
Async XLA Ops:
  0.0 1.6 %copy-start = (bf16[512,2048]{1,0:T(8,128)(2,1)S(1)}, bf16[512,2048]{1,0:T(8,128)(2,1)}, u32[]{:S(2)}) copy-start(bf16[512,2048]{1,0:T(8,128)(2,1)} %param.13) | copy-start | bytes 6291460
  5.7 22.9 %all-to-all-start = ((bf16[32,16,512]{2,1,0:T(8,128)(2,1)}), bf16[32,16,512]{2,1,0:T(8,128)(2,1)S(1)}, u32[]{:S(2)}, u32[]{:S(2)}) async-start(bf16[32,16,512]{2,1,0:T(8,128)(2,1)} %bitcast.2), calls=%async_computation | async-start | bytes 1048576 | tf_op jit(solution)/shard_map/all_to_all | solution.py:143
  28.6 0.8 %copy-start.1 = (bf16[32,16,512]{2,1,0:T(8,128)(2,1)}, bf16[32,16,512]{2,1,0:T(8,128)(2,1)S(1)}, u32[]{:S(2)}) copy-start(bf16[32,16,512]{2,1,0:T(8,128)(2,1)S(1)} %all-to-all-done) | copy-start | bytes 1572868
  34.4 18.6 %all-to-all-start.1 = ((bf16[32,16,512]{2,1,0:T(8,128)(2,1)}), bf16[32,16,512]{2,1,0:T(8,128)(2,1)S(1)}, u32[]{:S(2)}, u32[]{:S(2)}) async-start(bf16[32,16,512]{2,1,0:T(8,128)(2,1)} %bitcast.16), calls=%async_computation.1 | async-start | bytes 1048576 | tf_op jit(solution)/shard_map/all_to_all | solution.py:163
  37.4 15.6 %copy-start.2 = (f32[2048]{0:T(1024)S(1)}, f32[2048]{0:T(1024)}, u32[]{:S(2)}) copy-start(f32[2048]{0:T(1024)} %param.16) | copy-start | bytes 24580
  37.4 15.6 %copy-start.3 = (bf16[512,512]{1,0:T(8,128)(2,1)S(1)}, bf16[512,512]{1,0:T(8,128)(2,1)}, u32[]{:S(2)}) copy-start(bf16[512,512]{1,0:T(8,128)(2,1)} %constant.52.clone) | copy-start | bytes 1572868

commit v2 on v1

--- a/solution.py
+++ b/solution.py
@@ -12,6 +12,9 @@
 GROUP_DIM = 64
 LANES = 128
 AXES = ("row", "col")
+TILE = 512
+NEARLY = 125 << 19
+WHOLE = 62 << 20
 
 
 def wave(left, right, period):
@@ -76,14 +79,37 @@
     return first, cos_t, sin_t, last, lane_perm, row_perm
 
 
-def length_kernel(n_dev, slots, flag_ref, x_ref, first_ref, cos_ref, sin_ref, last_ref, lane_ref, row_ref, out_ref, z_ref, a_ref, b_ref):
+def length_kernel(n_dev, slots, x_hbm, first_hbm, cos_hbm, sin_hbm, last_hbm, lane_hbm, row_hbm, out_ref, z_ref, a_ref, b_ref, x_ref, cos_ref, sin_ref, first_ref, last_ref, lane_ref, row_ref, sem):
     rows, lanes = x_ref.shape
     pairs = slots // 2
     f32 = jnp.float32
+    upper, lower = pl.ds(0, rows), pl.ds(rows, rows)
+    loads = [
+        pltpu.make_async_copy(source, target, sem.at[i])
+        for i, (source, target) in enumerate(
+            (
+                (first_hbm.at[upper, :], first_ref.at[upper, :]),
+                (first_hbm.at[lower, :], first_ref.at[lower, :]),
+                (last_hbm, last_ref),
+                (lane_hbm, lane_ref),
+                (row_hbm, row_ref),
+                (x_hbm, x_ref),
+                (cos_hbm, cos_ref),
+                (sin_hbm, sin_ref),
+            )
+        )
+    ]
+    for i in (5, 0, 1, 6, 7, 2, 3, 4):
+        loads[i].start()
+    loads[5].wait()
+    loads[0].wait()
     y_re = jnp.dot(first_ref[:rows, :], x_ref[...], preferred_element_type=f32)
+    loads[1].wait()
     y_im = jnp.dot(first_ref[rows:, :], x_ref[...], preferred_element_type=f32)
+    loads[6].wait()
+    loads[7].wait()
     cos_t, sin_t = cos_ref[...], sin_ref[...]
-    flag = flag_ref[0]
+    flag = (lax.axis_index(AXES) * pairs % (GROUP_DIM // 2) == 0).astype(f32)
     for slot in range(slots):
         if slot < pairs:
             t_re, t_im = cos_t, -sin_t
@@ -96,6 +122,7 @@
         p_re, p_im = y_re[here, :], y_im[here, :]
         z_ref[here, :lanes] = (p_re * t_re - p_im * t_im).astype(jnp.bfloat16)
         z_ref[here, lanes:] = (p_re * t_im + p_im * t_re).astype(jnp.bfloat16)
+    loads[2].wait()
     spec = lax.dot_general(last_ref[...], z_ref[...], (((1,), (1,)), ((), ())), preferred_element_type=f32)
     spec = spec.astype(jnp.bfloat16)
     blocks = lanes // LANES
@@ -106,6 +133,7 @@
                 v * tall : (v + 1) * tall, e * LANES : (e + 1) * LANES
             ]
     f_n = slots // blocks
+    loads[3].wait()
     if f_n > 1:
         mixed = jnp.dot(a_ref[...], lane_ref[...], preferred_element_type=f32).astype(jnp.bfloat16)
         wide = lanes // f_n
@@ -119,7 +147,68 @@
         ordered = b_ref[...]
     else:
         ordered = a_ref[...]
+    loads[4].wait()
     out_ref[...] = jnp.dot(row_ref[...], ordered, preferred_element_type=f32).astype(jnp.bfloat16)
+
+
+def project_kernel(steps, tokens_ref, w_ref, forward_ref, out_ref, t_ref, m_ref, sem):
+    deep = w_ref.shape[0] // steps
+    copies = []
+    for k in range(steps):
+        part = pl.ds(k * deep, deep)
+        pair = (
+            pltpu.make_async_copy(tokens_ref.at[:, part], t_ref.at[:, part], sem.at[0, k]),
+            pltpu.make_async_copy(w_ref.at[part, :], m_ref.at[part, :], sem.at[1, k]),
+        )
+        for copy in pair:
+            copy.start()
+        copies.append(pair)
+    total = None
+    for k in range(steps):
+        for copy in copies[k]:
+            copy.wait()
+        part = pl.ds(k * deep, deep)
+        term = jnp.dot(t_ref[:, part], m_ref[part, :], preferred_element_type=jnp.float32)
+        total = term if total is None else total + term
+    mixed_in = total.astype(jnp.bfloat16)
+    for low in range(0, out_ref.shape[0], LANES):
+        out_ref[low : low + LANES, :] = lax.dot_general(
+            forward_ref[...],
+            mixed_in[:, low : low + LANES],
+            (((0,), (1,)), ((), ())),
+            preferred_element_type=jnp.float32,
+        ).astype(jnp.bfloat16)
+
+
+def branch_kernel(tiles, back_ref, combine_ref, gate_hbm, w_hbm, out_hbm, g_ref, w_ref, o_ref, spectrum_ref, sem):
+    wide = w_ref.shape[1] // tiles
+    parts = [pl.ds(i * wide, wide) for i in range(tiles)]
+    loads = [
+        (
+            pltpu.make_async_copy(w_hbm.at[:, part], w_ref.at[:, part], sem.at[0, i]),
+            pltpu.make_async_copy(gate_hbm.at[:, part], g_ref.at[:, part], sem.at[1, i]),
+        )
+        for i, part in enumerate(parts)
+    ]
+    stores = [pltpu.make_async_copy(o_ref.at[:, part], out_hbm.at[:, part], sem.at[2, i]) for i, part in enumerate(parts)]
+    for pair in loads:
+        for load in pair:
+            load.start()
+    for low in range(0, back_ref.shape[0], LANES):
+        spectrum_ref[:, low : low + LANES] = lax.dot_general(
+            back_ref[low : low + LANES, :],
+            combine_ref[...],
+            (((0,), (0,)), ((), ())),
+            preferred_element_type=jnp.float32,
+        ).astype(jnp.bfloat16)
+    for part, pair, store in zip(parts, loads, stores):
+        for load in pair:
+            load.wait()
+        branch = jnp.dot(spectrum_ref[...], w_ref[:, part], preferred_element_type=jnp.float32)
+        o_ref[:, part] = (g_ref[:, part].astype(jnp.float32) * branch).astype(jnp.bfloat16)
+        store.start()
+    for store in stores:
+        store.wait()
 
 
 def shards(tokens, w_mix, w_gate, gate_bias, w_branch):
@@ -136,39 +225,78 @@
     first, cos_t, sin_t, last, lane_perm, row_perm = (
         jnp.asarray(t, dtype) for t, dtype in zip(tables, (bf16, f32, f32, bf16, bf16, bf16))
     )
-    mixed_in = jnp.dot(tokens, w_mix, preferred_element_type=f32).astype(bf16)
-    slotted = lax.dot_general(
-        jnp.asarray(forward, bf16), mixed_in, (((0,), (1,)), ((), ())), preferred_element_type=f32
-    ).astype(bf16)
+    forward, combine = (jnp.asarray(t[:LANES, :LANES], bf16) for t in (forward, combine))
+    depth = w_mix.shape[0]
+    vmem = pl.BlockSpec(memory_space=pltpu.VMEM)
+    hbm = pl.BlockSpec(memory_space=pltpu.HBM)
+    steps = max(1, depth // TILE)
+    slotted = pl.pallas_call(
+        functools.partial(project_kernel, steps),
+        out_shape=jax.ShapeDtypeStruct((channels, local_len), bf16),
+        in_specs=[hbm, hbm, vmem],
+        out_specs=vmem,
+        scratch_shapes=[
+            pltpu.VMEM(tokens.shape, bf16),
+            pltpu.VMEM(w_mix.shape, bf16),
+            pltpu.SemaphoreType.DMA((2, steps)),
+        ],
+        compiler_params=pltpu.CompilerParams(vmem_limit_bytes=WHOLE),
+        cost_estimate=pl.CostEstimate(
+            flops=2 * local_len * depth * channels, bytes_accessed=2 * depth * (local_len + channels), transcendentals=0
+        ),
+        name="project",
+    )(tokens, w_mix, forward)
     pieces = lax.all_to_all(
         slotted.reshape(n_dev, slots, local_len), AXES, split_axis=0, concat_axis=0, tiled=True
     ).reshape(channels, local_len)
-    flag = (lax.axis_index(AXES) * pairs % (GROUP_DIM // 2) == 0).astype(f32).reshape(1)
-    vmem = pl.BlockSpec(memory_space=pltpu.VMEM)
     spectra = pl.pallas_call(
         functools.partial(length_kernel, n_dev, slots),
         out_shape=jax.ShapeDtypeStruct((channels, local_len), bf16),
-        in_specs=[pl.BlockSpec(memory_space=pltpu.SMEM)] + [vmem] * 7,
+        in_specs=[hbm] * 7,
         out_specs=vmem,
         scratch_shapes=[
             pltpu.VMEM((channels, 2 * local_len), bf16),
             pltpu.VMEM((channels, local_len), bf16),
             pltpu.VMEM((channels, local_len), bf16),
+            pltpu.VMEM((channels, local_len), bf16),
+            pltpu.VMEM(cos_t.shape, f32),
+            pltpu.VMEM(sin_t.shape, f32),
+            pltpu.VMEM(first.shape, bf16),
+            pltpu.VMEM(last.shape, bf16),
+            pltpu.VMEM(lane_perm.shape, bf16),
+            pltpu.VMEM(row_perm.shape, bf16),
+            pltpu.SemaphoreType.DMA((8,)),
         ],
         cost_estimate=pl.CostEstimate(
             flops=12 * channels * local_len * local_len, bytes_accessed=6 << 20, transcendentals=0
         ),
+        compiler_params=pltpu.CompilerParams(vmem_limit_bytes=NEARLY),
         name="length_transform",
-    )(flag, pieces, first, cos_t, sin_t, last, lane_perm, row_perm)
+    )(pieces, first, cos_t, sin_t, last, lane_perm, row_perm)
     back = lax.all_to_all(
         spectra.reshape(n_dev, slots, local_len), AXES, split_axis=0, concat_axis=0, tiled=True
     ).reshape(channels, local_len)
-    gate = jax.nn.sigmoid(jnp.dot(tokens, w_gate, preferred_element_type=f32) + gate_bias)
-    spectrum = lax.dot_general(
-        back, jnp.asarray(combine, bf16), (((0,), (0,)), ((), ())), preferred_element_type=f32
-    ).astype(bf16)
-    branch = jnp.dot(spectrum, w_branch, preferred_element_type=f32)
-    return (gate * branch).astype(bf16)
+    width = w_branch.shape[1]
+    tiles = max(1, width // TILE)
+    gate = jax.nn.sigmoid(jnp.dot(tokens, w_gate, preferred_element_type=f32) + gate_bias).astype(bf16)
+    return pl.pallas_call(
+        functools.partial(branch_kernel, tiles),
+        out_shape=jax.ShapeDtypeStruct((local_len, width), bf16),
+        in_specs=[vmem, vmem, hbm, hbm],
+        out_specs=hbm,
+        scratch_shapes=[
+            pltpu.VMEM((local_len, width), bf16),
+            pltpu.VMEM((channels, width), bf16),
+            pltpu.VMEM((local_len, width), bf16),
+            pltpu.VMEM((local_len, channels), bf16),
+            pltpu.SemaphoreType.DMA((3, tiles)),
+        ],
+        compiler_params=pltpu.CompilerParams(vmem_limit_bytes=WHOLE),
+        cost_estimate=pl.CostEstimate(
+            flops=2 * local_len * channels * width, bytes_accessed=6 * local_len * width, transcendentals=0
+        ),
+        name="branch",
+    )(back, combine, gate, w_branch)
 
 
 def solution(mesh):

time: 58.7 us -> 57.5 us (0.980)
  blocking collectives: 0 us -> 23.1 us
  waiting for transfers between devices: 21.8 us -> 5.33 us
  Pallas kernels: 5 us -> 14.6 us
  matrix products: 18.8 us -> 10.3 us
  starting transfers between devices: 10.3 us -> 2.98 us
  local copies, waits for them, and re-layouts: 2.4 us -> 0.8 us
    all_to_all x0 -> x1, blocking collectives: none -> 23.1 us  [shards(): lax.all_to_all(slotted.reshape(n_dev, slots, local_len), AXES, split_axis...]
    all_to_all x1 -> x0, waiting for transfers between devices: 15.6 us -> none  [shards(): lax.all_to_all(slotted.reshape(n_dev, slots, local_len), AXES, split_axis...]
    pallas_call x0 -> x2, Pallas kernels: none -> 9.68 us  [the longest x1 4.93 us: shards(): pl.pallas_call(functools.partial(branch_kernel, tiles), out_shape=jax.Sha...]
    dot_general x2 -> x0, matrix products: 9.37 us -> none  [the longest x1 5.27 us: shards(): branch = jnp.dot(spectrum, w_branch, preferred_element_type=f32)]
    all_to_all x1 -> x0, starting transfers between devices: 7.32 us -> none  [shards(): lax.all_to_all(slotted.reshape(n_dev, slots, local_len), AXES, split_axis...]
    unnamed x8 -> x4, local copies, waits for them, and re-layouts: 2.4 us -> 0.8 us
    dot_general x1, matrix products: 9.43 us -> 10.3 us  [shards(): jnp.dot(tokens, w_gate, preferred_element_type=f32) + gate_bias]
    all_to_all x1, waiting for transfers between devices: 6.16 us -> 5.33 us  [shards(): lax.all_to_all(spectra.reshape(n_dev, slots, local_len), AXES, split_axis...]
  transfers between devices with their start and end apart: 2 -> 1, of which waited for: 2 -> 1; matrix products, arithmetic and copies ran while one was open for 16% -> 18% of each run, Pallas kernels for 0% -> 0%
where the time goes in v2:
time: 57.5 us; the launch traced here: 57.1 us
  blocking collectives  23.1 us (40%)
  Pallas kernels  14.6 us (25%)
  matrix products  10.3 us (18%)
  waiting for transfers between devices  5.33 us (9%)
  starting transfers between devices  2.98 us (5%)
  local copies, waits for them, and re-layouts  0.8 us (1%)
    all_to_all x1, blocking collectives, shards(): lax.all_to_all(slotted.reshape(n_dev, slots, local_len), AXES, split_axis...  23.1 us
    dot_general x1, matrix products, shards(): jnp.dot(tokens, w_gate, preferred_element_type=f32) + gate_bias  10.3 us
    all_to_all x1, waiting for transfers between devices, shards(): lax.all_to_all(spectra.reshape(n_dev, slots, local_len), AXES, split_axis...  5.33 us
    pallas_call x1, Pallas kernels, shards(): pl.pallas_call(functools.partial(length_kernel, n_dev, slots), out_shape=...  4.93 us
    pallas_call x1, Pallas kernels, shards(): pl.pallas_call(functools.partial(branch_kernel, tiles), out_shape=jax.Sha...  4.93 us
    pallas_call x1, Pallas kernels, shards(): pl.pallas_call(functools.partial(project_kernel, steps), out_shape=jax.Sh...  4.75 us
    all_to_all x1, starting transfers between devices, shards(): lax.all_to_all(spectra.reshape(n_dev, slots, local_len), AXES, split_axis...  2.98 us
  transfers between devices with their start and end apart: 1, of which 1 were waited for; matrix products, arithmetic and copies ran while one was open for 18% of the time, Pallas kernels for 0%

profile of v2, /device:TPU:0, one launch (start us, length us, event | category | flops | bytes accessed | tf_op | source)
XLA Modules:
  0.0 57.1 jit_solution(4052683949832038569)
XLA Ops:
  0.0 4.8 %project.1 = bf16[512,512]{1,0:T(8,128)(2,1)} custom-call(bf16[512,2048]{1,0:T(8,128)(2,1)} %tokens_ref.1, bf16[2048,512]{1,0:T(8,128)(2,1)} %w_ref.1, bf16[128,128]{1,0:T(8,128)(2,1)} %constant.24.clone.forward_ref), custom_call_target="tpu_custom_call" | custom-call | flops 1073741824 | bytes 4194304 | tf_op jit(solution)/shard_map/project/pallas_call | solution.py:233
  4.8 0.0 copy-start.1
  4.8 23.1 %all_to_all.10 = bf16[32,16,512]{2,1,0:T(8,128)(2,1)} all-to-all(bf16[32,16,512]{2,1,0:T(8,128)(2,1)} %bitcast.6), channel_id=1, replica_groups=mesh['row'=8,'col'=4] {'row','col'}, dimensions={0} | all-to-all | bytes 1048576 | tf_op jit(solution)/shard_map/all_to_all | solution.py:249
  27.8 4.9 %length_transform.1 = bf16[512,512]{1,0:T(8,128)(2,1)} custom-call(bf16[512,512]{1,0:T(8,128)(2,1)} %bitcast.9, bf16[1024,512]{1,0:T(8,128)(2,1)} %constant.18.clone.first_hbm, f32[32,512]{1,0:T(8,128)} %constant.19.clone.cos_hbm, f32[32,512]{1,0:T(8,128)} %constant.20.clone.sin_hbm, bf16[512,1024]{1,0:T(8,128)(2,1)} %constant.21.clone.last_hbm, ...), custom_call_target="tpu_custom_call" | custom-call | flops 1610612736 | bytes 6291456 | tf_op jit(solution)/shard_map/length_transform/pallas_call | solution.py:252
  32.8 3.0 %all-to-all-start.1 = ((bf16[32,16,512]{2,1,0:T(8,128)(2,1)}), bf16[32,16,512]{2,1,0:T(8,128)(2,1)S(1)}, u32[]{:S(2)}, u32[]{:S(2)}) async-start(bf16[32,16,512]{2,1,0:T(8,128)(2,1)} %bitcast.8), calls=%async_computation.1 | async-start | bytes 1048576 | tf_op jit(solution)/shard_map/all_to_all | solution.py:276
  35.8 0.0 copy-done.1
  35.8 10.3 %divide_convert_fusion.gate_hbm = bf16[512,2048]{1,0:T(8,128)(2,1)} fusion(bf16[512,2048]{1,0:T(8,128)(2,1)} %tokens_ref.1, bf16[2048,2048]{1,0:T(8,128)(2,1)} %param.15, f32[2048]{0:T(1024)S(1)} %copy-done.1), kind=kOutput, calls=%fused_computation | convolution fusion | flops 4300210176 | bytes 12591104 | tf_op jit(solution)/shard_map/dot_general | solution.py:281
  46.0 5.3 %all-to-all-done.1 = bf16[32,16,512]{2,1,0:T(8,128)(2,1)S(1)} async-done(((bf16[32,16,512]{2,1,0:T(8,128)(2,1)}), bf16[32,16,512]{2,1,0:T(8,128)(2,1)S(1)}, u32[]{:S(2)}, u32[]{:S(2)}) %all-to-all-start.1) | async-done | bytes 524320 | tf_op jit(solution)/shard_map/all_to_all | solution.py:276
  51.4 0.0 copy-start
  51.4 0.8 %copy-done = bf16[32,16,512]{2,1,0:T(8,128)(2,1)} copy-done((bf16[32,16,512]{2,1,0:T(8,128)(2,1)}, bf16[32,16,512]{2,1,0:T(8,128)(2,1)S(1)}, u32[]{:S(2)}) %copy-start) | copy-done | bytes 524312
  52.2 4.9 %branch.1 = bf16[512,2048]{1,0:T(8,128)(2,1)} custom-call(bf16[512,512]{1,0:T(8,128)(2,1)} %bitcast.7, bf16[128,128]{1,0:T(8,128)(2,1)} %constant.25.clone.combine_ref, bf16[512,2048]{1,0:T(8,128)(2,1)} %divide_convert_fusion.gate_hbm, bf16[512,2048]{1,0:T(8,128)(2,1)} %w_hbm.1), custom_call_target="tpu_custom_call" | custom-call | flops 1073741824 | bytes 6291456 | tf_op jit(solution)/shard_map/branch/pallas_call | solution.py:282
Async XLA Ops:
  4.8 31.0 %copy-start.1 = (f32[2048]{0:T(1024)S(1)}, f32[2048]{0:T(1024)}, u32[]{:S(2)}) copy-start(f32[2048]{0:T(1024)} %param.16) | copy-start | bytes 24580
  32.8 18.6 %all-to-all-start.1 = ((bf16[32,16,512]{2,1,0:T(8,128)(2,1)}), bf16[32,16,512]{2,1,0:T(8,128)(2,1)S(1)}, u32[]{:S(2)}, u32[]{:S(2)}) async-start(bf16[32,16,512]{2,1,0:T(8,128)(2,1)} %bitcast.8), calls=%async_computation.1 | async-start | bytes 1048576 | tf_op jit(solution)/shard_map/all_to_all | solution.py:276
  51.4 0.8 %copy-start = (bf16[32,16,512]{2,1,0:T(8,128)(2,1)}, bf16[32,16,512]{2,1,0:T(8,128)(2,1)S(1)}, u32[]{:S(2)}) copy-start(bf16[32,16,512]{2,1,0:T(8,128)(2,1)S(1)} %all-to-all-done.1) | copy-start | bytes 1572868
